TPU v7x, 512 devices: a whole 4x8x8 slice. The times are simulated.
512 devices in a mesh: sp: 32 (over z, x), tp: 16 (over y, core).
Axes of the slice: x: 4, y: 8, z: 8, core: 2. Of those that a mesh axis runs over, the one named last changes fastest.
Arguments:
- resid: bfloat16 [16384, 2048], P(('sp', 'tp')), may hold values from -6 to 6
- recurrent_input: bfloat16 [16384, 2048], P('sp', 'tp'), may hold values from -12.2 to 12.2
- recurrent_out_gate: bfloat16 [16384, 2048], P('sp', 'tp'), may hold values from -6 to 6
- filter_weight: float32 [4, 2048], P(None, 'tp'), may hold values from -3 to 3
- recurrence_gate_matrix: bfloat16 [32, 64, 64], P('tp'), may hold values from -0.75 to 0.75
- input_gate_matrix: bfloat16 [32, 64, 64], P('tp'), may hold values from -0.75 to 0.75
- channel_decay_raw: float32 [2048], P('tp'), may hold values from 4.8 to 13.5
- token_decay_boost: float32 [16384, 2048], P('sp', 'tp'), may hold values from -0.7 to 0
- output_projection_weight: bfloat16 [2048, 2048], P('tp'), may hold values from -0.375 to 0.375
- expert_norm_gain: float32 [2048], replicated, may hold values from 0.1 to 1.9
- routes: int32 [16384, 2], P('sp'), may hold values from 0 to 31, all different within a row; in each aligned block of 32 rows (0 to 31, 32 to 63, ...) at most 3 rows name the same one
- expert_pair_weight: float32 [16384, 2], P(('sp', 'tp')), may hold values from 0.2 to 0.8
- gate_weight: bfloat16 [32, 2048, 2048], P('sp', None, 'tp'), may hold values from -0.125 to 0.125
- up_weight: bfloat16 [32, 2048, 2048], P('sp', None, 'tp'), may hold values from -0.125 to 0.125
- down_weight: bfloat16 [32, 2048, 2048], P('sp', None, 'tp'), may hold values from -0.25 to 0.25
Outputs:
- layer_out: bfloat16 [16384, 2048], P(('sp', 'tp'))
Inputs may be any that keep to these rules, and one draw needn't show every extreme that they name: `routes`: in each aligned block of 32 rows no expert is named by more than 3 rows, and the two experts of a row differ.
All inputs are finite; a program needn't handle non-finite values.
Results may differ from a plain program's by a relative error of at most 0.013.
Values may be sent and summed in bfloat16 or wider, within the bound.
No kernel may reach another device: no remote copies, remote signals or barrier semaphores. Data moves between devices by JAX's collectives and lax.ppermute only.
A program may use at most 64 MiB of HBM per device.

v0:
```python
import jax
import jax.numpy as jnp
from jax import lax
from jax.sharding import PartitionSpec as P

RECURRENT_SCALE = 8.0
EPSILON = 1e-06


def shifted(block, axis, distance):
    devices = range(lax.axis_size(axis))
    route = [(i - distance, i) for i in devices if i - distance in devices]
    return lax.ppermute(block, axis, route)


def from_everyone(x, axis):
    size = lax.axis_size(axis)
    return lax.all_to_all(jnp.broadcast_to(x[None], (size, *x.shape)), axis, 0, 0, tiled=True)


def collected_together(x, axis):
    leaves = jax.tree.leaves(x)
    order = sorted(range(len(leaves)), key=lambda k: -leaves[k].size)
    width = (1, *leaves[order[0]].shape)[-1]
    lines = [
        jnp.pad(leaves[k].reshape(-1), (0, -leaves[k].size % width)).reshape(-1, width)
        for k in order
    ]
    both, at, found = (from_everyone(jnp.concatenate(lines), axis), 0, {})
    for k, line in zip(order, lines):
        slab = both[:, at : at + len(line)].reshape(len(both), -1)
        found[k] = slab[:, : leaves[k].size].reshape(-1, *leaves[k].shape)
        at += len(line)
    numbers = iter(range(len(leaves)))
    return jax.tree.map(lambda _: found[next(numbers)], x)


def joined_by_halves(pieces, combine):
    while len(jax.tree.leaves(pieces)[0]) > 1:
        pieces = jax.vmap(combine)(
            *(jax.tree.map(lambda part: part[side::2], pieces) for side in (0, 1))
        )
    return jax.tree.map(lambda part: part[0], pieces)


def carried_in(x, axis, combine, identity):
    size, position = (lax.axis_size(axis), lax.axis_index(axis))
    passed = jnp.arange(size) < position

    def kept(part, zero, own):
        part = jnp.where(
            passed.reshape(-1, *(1 for _ in own.shape)), part, jnp.asarray(zero, own.dtype)
        )
        return part

    pieces = collected_together(x, axis)
    return joined_by_halves(jax.tree.map(kept, pieces, identity, x), combine)


def split_up(x, dim, size):
    before, after = (x.shape[:dim], x.shape[dim + 1 :])
    return jnp.moveaxis(x.reshape(*before, size, -1, *after), dim, 0)


def sum_at_owner(x, axis, dim):
    pieces = split_up(x, dim, lax.axis_size(axis))
    arrived = lax.all_to_all(pieces, axis, split_axis=0, concat_axis=0, tiled=True)
    return arrived.astype(jnp.float32).sum(axis=0)


def in_order(pieces, dim):
    pieces = jnp.moveaxis(pieces, 0, dim)
    dims = pieces.shape
    return pieces.reshape(*dims[:dim], dims[dim] * dims[dim + 1], *dims[dim + 2 :])


def piecewise(x, axis, dim, work, out_dim):
    extent = x.shape[dim]
    pieces = jnp.split(x, 2, axis=dim) if extent % 2 == 0 else [x]
    first = jnp.arange(lax.axis_size(axis)) * extent
    blocks = [lax.all_gather(slab, axis) for slab in pieces]
    made = [jax.vmap(work)(b, first + k * (extent // len(pieces))) for k, b in enumerate(blocks)]
    return in_order(jnp.concatenate(made, axis=out_dim + 1), out_dim)


def chain_step(earlier, later):
    return (earlier[0] * later[0], later[0] * earlier[1] + later[1])


def slot_numbers(picks, experts):
    flat = picks.reshape(-1)
    onehot = (flat[:, None] == jnp.arange(experts, dtype=jnp.int32)[None, :]).astype(jnp.int32)
    before = jnp.cumsum(onehot, axis=0) - onehot
    return (flat, jnp.sum(before * onehot, axis=1))


def fill_slots(source_rows, slot_of, row_of, slot_count):
    match = slot_of[None, :] == jnp.arange(slot_count, dtype=jnp.int32)[:, None]
    picked = jnp.sum(jnp.where(match, row_of[None, :], 0), axis=1)
    present = jnp.any(match, axis=1)
    return jnp.where(present[:, None], source_rows[picked], jnp.zeros((), source_rows.dtype))


def expert_hidden(rows, gate_weight, up_weight):
    gate = jnp.dot(rows, gate_weight[0], preferred_element_type=jnp.float32)
    upward = jnp.dot(rows, up_weight[0], preferred_element_type=jnp.float32)
    return (jax.nn.silu(gate) * upward).astype(jnp.bfloat16)


def expert_down(active, down_weight):
    columns = down_weight[0]
    return jnp.dot(
        lax.all_gather(active, "tp", axis=1, tiled=True),
        columns,
        preferred_element_type=jnp.float32,
    ).astype(jnp.bfloat16)


def body(
    resid,
    recurrent_input,
    recurrent_out_gate,
    filter_weight,
    recurrence_gate_matrix,
    input_gate_matrix,
    channel_decay_raw,
    token_decay_boost,
    output_projection_weight,
    expert_norm_gain,
    routes,
    expert_pair_weight,
    gate_weight,
    up_weight,
    down_weight,
):
    tokens_here, channels = recurrent_input.shape
    taps = filter_weight.shape[0]
    rim = shifted(recurrent_input[tokens_here - taps + 1 :], "sp", 1)
    extended = jnp.concatenate([rim, recurrent_input], axis=0).astype(jnp.float32)
    mixed_in = extended[0:tokens_here] * filter_weight[0]
    for offset in range(1, taps):
        mixed_in = mixed_in + extended[offset : offset + tokens_here] * filter_weight[offset]
    smoothed = mixed_in.astype(jnp.bfloat16)
    grouped = smoothed.reshape(
        tokens_here, recurrence_gate_matrix.shape[0], recurrence_gate_matrix.shape[1]
    )
    recurrence_gate = jax.nn.sigmoid(
        jnp.einsum(
            "tni,nij->tnj", grouped, recurrence_gate_matrix, preferred_element_type=jnp.float32
        ).reshape(tokens_here, channels)
    )
    input_gate = jax.nn.sigmoid(
        jnp.einsum(
            "tni,nij->tnj", grouped, input_gate_matrix, preferred_element_type=jnp.float32
        ).reshape(tokens_here, channels)
    )
    decay_logarithm = (
        -RECURRENT_SCALE * recurrence_gate * jax.nn.softplus(-channel_decay_raw) + token_decay_boost
    )
    decay = jnp.exp(decay_logarithm)
    drive = jnp.sqrt(-jnp.expm1(2.0 * decay_logarithm)) * (
        input_gate * smoothed.astype(jnp.float32)
    )
    running, local_state = lax.associative_scan(chain_step, (decay, drive), axis=0)
    identity = (jnp.ones((channels,), jnp.float32), jnp.zeros((channels,), jnp.float32))
    carried = carried_in((running[-1], local_state[-1]), "sp", chain_step, identity)
    state = local_state + running * carried[1][None, :]
    branch = (jax.nn.gelu(recurrent_out_gate.astype(jnp.float32)) * state).astype(jnp.bfloat16)
    tp_size = lax.axis_size("tp")
    rows_dev = tokens_here // tp_size
    projected = sum_at_owner(
        jnp.dot(branch, output_projection_weight, preferred_element_type=jnp.float32).astype(
            jnp.bfloat16
        ),
        "tp",
        0,
    )
    stream = (resid.astype(jnp.float32) + projected).astype(jnp.bfloat16)
    stream_wide = stream.astype(jnp.float32)
    normed = (
        stream_wide
        * lax.rsqrt(jnp.mean(stream_wide * stream_wide, axis=1, keepdims=True) + EPSILON)
        * expert_norm_gain
    ).astype(jnp.bfloat16)
    model_width = normed.shape[1]
    experts = lax.axis_size("sp")
    capacity = max(2, 3 * rows_dev // experts)
    own_routes = lax.dynamic_slice_in_dim(routes, lax.axis_index("tp") * rows_dev, rows_dev, 0)
    own_flat, own_rank = slot_numbers(own_routes, experts)
    own_slots = own_flat * capacity + own_rank
    row_of = jnp.arange(2 * rows_dev, dtype=jnp.int32) // 2
    outgoing = fill_slots(normed, own_slots, row_of, experts * capacity).reshape(
        experts, capacity, model_width
    )
    arrived = lax.all_to_all(outgoing, "sp", split_axis=0, concat_axis=0, tiled=True)

    def hidden_piece(piece, start):
        flat_rows = piece.reshape(piece.shape[0] * piece.shape[1], model_width)
        return expert_hidden(flat_rows, gate_weight, up_weight).reshape(
            piece.shape[0], piece.shape[1], -1
        )

    active = piecewise(
        arrived.reshape(1, experts * capacity, model_width), "tp", 0, hidden_piece, 0
    )
    result = expert_down(active.reshape(-1, active.shape[2]), down_weight)
    joined = lax.all_to_all(
        result.reshape(tp_size, experts * capacity, -1),
        "tp",
        split_axis=0,
        concat_axis=2,
        tiled=True,
    )
    returned = lax.all_to_all(
        joined.reshape(experts, capacity, model_width),
        "sp",
        split_axis=0,
        concat_axis=0,
        tiled=True,
    )
    picked = (
        returned.reshape(experts * capacity, model_width)[own_slots]
        .astype(jnp.float32)
        .reshape(rows_dev, 2, model_width)
    )
    blended = jnp.sum(picked * expert_pair_weight[:, :, None], axis=1)
    return (stream_wide + blended).astype(jnp.bfloat16)


def solution(mesh):
    placed = (
        P(("sp", "tp"), None),
        P("sp", "tp"),
        P("sp", "tp"),
        P(None, "tp"),
        P("tp", None, None),
        P("tp", None, None),
        P("tp"),
        P("sp", "tp"),
        P("tp", None),
        P(),
        P("sp", None),
        P(("sp", "tp"), None),
        P("sp", None, "tp"),
        P("sp", None, "tp"),
        P("sp", None, "tp"),
    )
    return jax.shard_map(
        body, mesh=mesh, in_specs=placed, out_specs=P(("sp", "tp"), None), check_vma=False
    )
```

profile of v0, /device:TPU:1, one launch (start us, length us, event | category | flops | bytes accessed | tf_op | source)
XLA Modules:
  0.0 395.7 jit_solution(9061123407506774359)
XLA Ops:
  7.4 3.9 collective-permute-start
  13.9 1.1 copy.87
  17.5 1.0 fusion.15
  19.0 4.5 %slice.371 = f32[256,128]{0,1:T(8,128)S(1)} slice(f32[512,128]{0,1:T(8,128)S(1)} %get-tuple-element.9), slice={[0:511:2], [0:128:1]} | slice | bytes 262144 | tf_op jit(solution)/shard_map/slice | solution.py:164
  23.5 4.5 %slice.372 = f32[256,128]{0,1:T(8,128)S(1)} slice(f32[512,128]{0,1:T(8,128)S(1)} %get-tuple-element.9), slice={[1:512:2], [0:128:1]} | slice | bytes 262144 | tf_op jit(solution)/shard_map/slice | solution.py:164
  27.9 4.5 %slice.370 = f32[256,128]{0,1:T(8,128)S(1)} slice(f32[512,128]{0,1:T(8,128)S(1)} %get-tuple-element.10), slice={[1:512:2], [0:128:1]} | slice | bytes 262144 | tf_op jit(solution)/shard_map/slice | solution.py:164
  32.4 5.0 %slice.374 = f32[256,128]{0,1:T(8,128)S(1)} slice(f32[512,128]{0,1:T(8,128)S(1)} %get-tuple-element.10), slice={[0:511:2], [0:128:1]} | slice | bytes 262144 | tf_op jit(solution)/shard_map/slice | solution.py:164
  37.5 2.2 slice.377
  39.7 2.2 slice.378
  41.9 2.2 slice.376
  44.1 2.2 slice.380
  46.3 1.1 slice.383
  47.5 1.2 slice.384
  48.6 1.2 slice.382
  49.8 1.1 slice.386
  60.3 1.1 slice.381
  61.5 1.1 slice.430
  62.6 2.2 slice.375
  64.8 2.2 slice.432
  67.1 4.5 %slice.369 = f32[255,128]{0,1:T(8,128)S(1)} slice(f32[512,128]{0,1:T(8,128)S(1)} %get-tuple-element.10), slice={[2:512:2], [0:128:1]} | slice | bytes 261120 | tf_op jit(solution)/shard_map/slice | solution.py:164
  71.5 4.9 %slice.434 = f32[255,128]{0,1:T(8,128)S(1)} slice(f32[512,128]{0,1:T(8,128)S(1)} %get-tuple-element.9), slice={[2:512:2], [0:128:1]} | slice | bytes 261120 | tf_op jit(solution)/shard_map/slice | solution.py:164
  84.9 1.1 pad.140
  86.0 1.1 pad.141
  87.2 1.1 pad.123
  88.4 1.1 pad.122
  89.7 2.2 pad.142
  91.9 2.2 pad.143
  94.1 4.5 %pad.145 = f32[512,128]{0,1:T(8,128)S(1)} pad(f32[256,128]{0,1:T(8,128)S(1)} %add.346, f32[]{:T(128)} %constant.25.clone.1), padding=1_0_1x0_0_0 | pad | bytes 393220 | tf_op jit(solution)/shard_map/pad | solution.py:164
  98.7 2.2 pad.124
  100.9 2.2 pad.125
  103.3 4.4 %pad.144 = f32[512,128]{0,1:T(8,128)S(1)} pad(f32[256,128]{0,1:T(8,128)S(1)} %pad_maximum_fusion.1, f32[]{:T(128)} %constant.25.clone.1), padding=0_1_1x0_0_0 | pad | bytes 393220 | tf_op jit(solution)/shard_map/pad | solution.py:164
  107.9 4.6 %pad.127 = f32[512,128]{0,1:T(8,128)S(1)} pad(f32[256,128]{0,1:T(8,128)S(1)} %add.336, f32[]{:T(128)} %constant.25.clone.1), padding=1_0_1x0_0_0 | pad | bytes 393220 | tf_op jit(solution)/shard_map/pad | solution.py:164
  112.6 4.4 %pad.126 = f32[512,128]{0,1:T(8,128)S(1)} pad(f32[256,128]{0,1:T(8,128)S(1)} %pad_maximum_fusion, f32[]{:T(128)} %constant.25.clone.1), padding=0_1_1x0_0_0 | pad | bytes 393220 | tf_op jit(solution)/shard_map/pad | solution.py:164
  117.8 12.6 %all-to-all-start = ((f32[32,2,128]{2,1,0:T(2,128)}), f32[32,2,128]{2,1,0:T(2,128)S(1)}, u32[]{:S(2)}, u32[]{:S(2)}) async-start(f32[32,2,128]{2,1,0:T(2,128)} %broadcast_in_dim.64), calls=%async_computation | async-start | bytes 65536 | tf_op jit(solution)/shard_map/all_to_all | solution.py:18
  130.4 8.7 %all-to-all-done = f32[32,2,128]{2,1,0:T(2,128)S(1)} async-done(((f32[32,2,128]{2,1,0:T(2,128)}), f32[32,2,128]{2,1,0:T(2,128)S(1)}, u32[]{:S(2)}, u32[]{:S(2)}) %all-to-all-start) | async-done | bytes 32800 | tf_op jit(solution)/shard_map/all_to_all | solution.py:18
  139.5 2.2 convolution_convert_fusion
  141.7 9.5 %all-to-all-start.1 = ((bf16[16,32,2048]{2,1,0:T(8,128)(2,1)}), bf16[16,32,2048]{2,1,0:T(8,128)(2,1)S(1)}, u32[]{:S(2)}, u32[]{:S(2)}) async-start(bf16[16,32,2048]{2,1,0:T(8,128)(2,1)} %bitcast.12), calls=%async_computation.1 | async-start | bytes 4194304 | tf_op jit(solution)/shard_map/all_to_all | solution.py:67
  152.9 47.3 %all-to-all-done.1 = bf16[16,32,2048]{2,1,0:T(8,128)(2,1)S(1)} async-done(((bf16[16,32,2048]{2,1,0:T(8,128)(2,1)}), bf16[16,32,2048]{2,1,0:T(8,128)(2,1)S(1)}, u32[]{:S(2)}, u32[]{:S(2)}) %all-to-all-start.1) | async-done | bytes 2097184 | tf_op jit(solution)/shard_map/all_to_all | solution.py:67
  202.3 19.6 %all_to_all.35 = bf16[32,3,2048]{2,1,0:T(4,128)(2,1)S(1)} all-to-all(bf16[32,3,2048]{2,1,0:T(4,128)(2,1)S(1)} %broadcast_select_fusion), channel_id=1, replica_groups=mesh['sp'=32,'tp'=16] {'sp'}, dimensions={0} | all-to-all | bytes 786432 | tf_op jit(solution)/shard_map/all_to_all | solution.py:195
  221.9 1.1 all_gather_reshape.3
  223.3 43.7 %all-gather.3.cloned.1.call-done = bf16[16,1,96,2048]{3,2,1,0:T(8,128)(2,1)} async-done(((bf16[1,1,96,2048]{3,2,1,0:T(8,128)(2,1)}), bf16[16,1,96,2048]{3,2,1,0:T(8,128)(2,1)}) %all-gather.3.cloned.1.call-update) | async-done | bytes 6291472 | tf_op jit(solution)/shard_map/all_gather | solution.py:81
  267.0 4.7 %fusion.2 = f32[16,96,128]{2,1,0:T(8,128)S(1)} fusion(bf16[16,1,96,2048]{3,2,1,0:T(8,128)(2,1)} %all-gather.3.cloned.1.call-done, bf16[1,2048,128]{2,1,0:T(8,128)(2,1)S(1)} %copy-done.5), kind=kOutput, calls=%fused_computation.4 | convolution fusion | flops 805306368 | bytes 7602176 | tf_op jit(solution)/shard_map/vmap()/dot_general | solution.py:105
  271.7 2.6 fusion.7
  274.4 58.5 %all-gather.5.cloned.1.call-done = bf16[1536,2048]{1,0:T(8,128)(2,1)} async-done(((bf16[1536,128]{1,0:T(8,128)(2,1)}), bf16[1536,2048]{1,0:T(8,128)(2,1)}) %all-gather.5.cloned.1.call-update) | async-done | bytes 6291472 | tf_op jit(solution)/shard_map/all_gather | solution.py:113
  332.9 4.6 %convolution_convert_fusion.1 = bf16[1536,128]{1,0:T(8,128)(2,1)S(1)} fusion(bf16[1536,2048]{1,0:T(8,128)(2,1)} %all-gather.5.cloned.1.call-done, bf16[1,2048,128]{2,1,0:T(8,128)(2,1)S(1)} %copy-done.7), kind=kOutput, calls=%fused_computation.8 | convolution fusion | flops 805502976 | bytes 7208960 | tf_op jit(solution)/shard_map/dot_general | solution.py:112
  337.5 19.4 %all_to_all.36 = bf16[16,96,128]{2,1,0:T(8,128)(2,1)S(1)} all-to-all(bf16[16,96,128]{2,1,0:T(8,128)(2,1)S(1)} %bitcast.97), channel_id=1, replica_groups=mesh['sp'=32,'tp'=16] {'tp'}, dimensions={0} | all-to-all | bytes 786432 | tf_op jit(solution)/shard_map/all_to_all | solution.py:207
  357.9 9.9 %all-to-all-start.4 = ((bf16[32,3,2048]{2,1,0:T(4,128)(2,1)}), bf16[32,3,2048]{2,1,0:T(4,128)(2,1)S(1)}, u32[]{:S(2)}, u32[]{:S(2)}) async-start(bf16[32,3,2048]{2,1,0:T(4,128)(2,1)} %reshape.148), calls=%async_computation.4 | async-start | bytes 1048576 | tf_op jit(solution)/shard_map/all_to_all | solution.py:214
  368.2 17.4 %all-to-all-done.4 = bf16[32,3,2048]{2,1,0:T(4,128)(2,1)S(1)} async-done(((bf16[32,3,2048]{2,1,0:T(4,128)(2,1)}), bf16[32,3,2048]{2,1,0:T(4,128)(2,1)S(1)}, u32[]{:S(2)}, u32[]{:S(2)}) %all-to-all-start.4) | async-done | bytes 393248 | tf_op jit(solution)/shard_map/all_to_all | solution.py:214
  (207 shorter events, 33.9 us)
Async XLA Ops:
  6.5 133.0 %copy-start = (bf16[128,2048]{1,0:T(8,128)(2,1)S(1)}, bf16[128,2048]{1,0:T(8,128)(2,1)}, u32[]{:S(2)}) copy-start(bf16[128,2048]{1,0:T(8,128)(2,1)} %param.23) | copy-start | bytes 1572868
  7.4 8.6 %collective-permute-start = (bf16[3,128]{0,1:T(8,128)(2,1)S(1)}, bf16[3,128]{0,1:T(8,128)(2,1)S(1)}, u32[]{:S(2)}, u32[]{:S(2)}) collective-permute-start(bf16[3,128]{0,1:T(8,128)(2,1)S(1)} %copy.84), channel_id=1, source_target_pairs={{0,16},{16,32},{32,48},{48,64},{64,80},{80,96},{96,112},{112,128},... | collective-permute-start | bytes 2312 | tf_op jit(solution)/shard_map/ppermute | solution.py:13
  107.8 92.8 %copy-start.1 = (bf16[32,2048]{1,0:T(8,128)(2,1)S(1)}, bf16[32,2048]{1,0:T(8,128)(2,1)}, u32[]{:S(2)}) copy-start(bf16[32,2048]{1,0:T(8,128)(2,1)} %param.15) | copy-start | bytes 393220
  112.4 88.3 %copy-start.2 = (f32[2048]{0:T(1024)S(1)}, f32[2048]{0:T(1024)}, u32[]{:S(2)}) copy-start(f32[2048]{0:T(1024)} %param.24) | copy-start | bytes 24580
  117.8 21.3 %all-to-all-start = ((f32[32,2,128]{2,1,0:T(2,128)}), f32[32,2,128]{2,1,0:T(2,128)S(1)}, u32[]{:S(2)}, u32[]{:S(2)}) async-start(f32[32,2,128]{2,1,0:T(2,128)} %broadcast_in_dim.64), calls=%async_computation | async-start | bytes 65536 | tf_op jit(solution)/shard_map/all_to_all | solution.py:18
  141.7 58.5 %all-to-all-start.1 = ((bf16[16,32,2048]{2,1,0:T(8,128)(2,1)}), bf16[16,32,2048]{2,1,0:T(8,128)(2,1)S(1)}, u32[]{:S(2)}, u32[]{:S(2)}) async-start(bf16[16,32,2048]{2,1,0:T(8,128)(2,1)} %bitcast.12), calls=%async_computation.1 | async-start | bytes 4194304 | tf_op jit(solution)/shard_map/all_to_all | solution.py:67
  151.2 115.8 %copy-start.5 = (bf16[1,2048,128]{2,1,0:T(8,128)(2,1)S(1)}, bf16[1,2048,128]{2,1,0:T(8,128)(2,1)}, u32[]{:S(2)}) copy-start(bf16[1,2048,128]{2,1,0:T(8,128)(2,1)} %param.27) | copy-start | bytes 1572868
  151.2 115.8 %all-gather.3.cloned.1.call-start = ((), (), s32[]{:S(2)}) async-start(), calls=%async_computation.5 | async-start | bytes 6684672 | tf_op jit(solution)/shard_map/all_gather | solution.py:81
  223.0 48.8 %copy-start.6 = (bf16[1,2048,128]{2,1,0:T(8,128)(2,1)S(1)}, bf16[1,2048,128]{2,1,0:T(8,128)(2,1)}, u32[]{:S(2)}) copy-start(bf16[1,2048,128]{2,1,0:T(8,128)(2,1)} %param.28) | copy-start | bytes 1572868
  223.0 109.9 %all-gather.5.cloned.1.call-start = ((), (), s32[]{:S(2)}) async-start(), calls=%async_computation.6 | async-start | bytes 6684672 | tf_op jit(solution)/shard_map/all_gather | solution.py:113
  267.0 4.8 %copy-start.4 = (bf16[16,1,96,2048]{3,2,1,0:T(8,128)(2,1)S(1)}, bf16[16,1,96,2048]{3,2,1,0:T(8,128)(2,1)}, u32[]{:S(2)}) copy-start(bf16[16,1,96,2048]{3,2,1,0:T(8,128)(2,1)} %all-gather.3.cloned.1.call-done) | copy-start | bytes 18874372
  271.7 61.1 %copy-start.7 = (bf16[1,2048,128]{2,1,0:T(8,128)(2,1)S(1)}, bf16[1,2048,128]{2,1,0:T(8,128)(2,1)}, u32[]{:S(2)}) copy-start(bf16[1,2048,128]{2,1,0:T(8,128)(2,1)} %param.29) | copy-start | bytes 1572868
  274.3 93.7 %copy-start.3 = (f32[32,2]{0,1:T(2,128)S(1)}, f32[32,2]{0,1:T(2,128)}, u32[]{:S(2)}) copy-start(f32[32,2]{0,1:T(2,128)} %param.26) | copy-start | bytes 772
  357.9 27.6 %all-to-all-start.4 = ((bf16[32,3,2048]{2,1,0:T(4,128)(2,1)}), bf16[32,3,2048]{2,1,0:T(4,128)(2,1)S(1)}, u32[]{:S(2)}, u32[]{:S(2)}) async-start(bf16[32,3,2048]{2,1,0:T(4,128)(2,1)} %reshape.148), calls=%async_computation.4 | async-start | bytes 1048576 | tf_op jit(solution)/shard_map/all_to_all | solution.py:214
Sparse Core Ops, SparseCore 0:
  223.1 43.8 all-gather.2
  274.5 58.3 all-gather.4
where the time goes:
time: 403 us; the launch traced here: 396 us
  waiting for transfers between devices  176 us (44%)
  local copies, waits for them, and re-layouts  105 us (26%)
  blocking collectives  39 us (10%)
  starting transfers between devices  36.2 us (9%)
  matrix products  16.1 us (4%)
  between operations  15.1 us (4%)
  other arithmetic  8.3 us (2%)
    all_gather x1, waiting for transfers between devices, expert_down(): lax.all_gather(active, 'tp', axis=1, tiled=True)  58.5 us
    slice x50, local copies, waits for them, and re-layouts, body(): lax.associative_scan(chain_step, (decay, drive), axis=0)  56 us
    all_to_all x1, waiting for transfers between devices, sum_at_owner(): lax.all_to_all(pieces, axis, split_axis=0, concat_axis=0, tiled=True)  47.3 us
    all_gather x1, waiting for transfers between devices, piecewise(): blocks = [lax.all_gather(slab, axis) for slab in pieces]  43.7 us
    pad x32, local copies, waits for them, and re-layouts, body(): lax.associative_scan(chain_step, (decay, drive), axis=0)  36.4 us
    all_to_all x1, blocking collectives, body(): lax.all_to_all(outgoing, 'sp', split_axis=0, concat_axis=0, tiled=True)  19.6 us
    all_to_all x1, blocking collectives, body(): lax.all_to_all(result.reshape(tp_size, experts * capacity, -1), 'tp', spl...  19.4 us
    all_to_all x1, waiting for transfers between devices, body(): lax.all_to_all(joined.reshape(experts, capacity, model_width), 'sp', spli...  17.4 us
  transfers between devices with their start and end apart: 6, of which 5 were waited for; matrix products, arithmetic and copies ran while one was open for 2% of the time, Pallas kernels for 0%

commit v1 on v0

--- a/solution.py
+++ b/solution.py
@@ -110,7 +110,7 @@
 def expert_down(active, down_weight):
     columns = down_weight[0]
     return jnp.dot(
-        lax.all_gather(active, "tp", axis=1, tiled=True),
+        jnp.concatenate(lax.all_gather(active, "tp"), axis=1),
         columns,
         preferred_element_type=jnp.float32,
     ).astype(jnp.bfloat16)

time: 403 us -> 400 us (level)
  waiting for transfers between devices: 176 us -> 165 us
  local copies, waits for them, and re-layouts: 105 us -> 114 us
    all_gather x1, waiting for transfers between devices: 58.5 us -> 47.6 us  [expert_down(): lax.all_gather(active, 'tp')]
    all_gather x0 -> x1, local copies, waits for them, and re-layouts: none -> 8.64 us  [expert_down(): lax.all_gather(active, 'tp')]
where the time goes in v1:
time: 400 us; the launch traced here: 393 us
  waiting for transfers between devices  165 us (41%)
  local copies, waits for them, and re-layouts  114 us (28%)
  blocking collectives  38.5 us (10%)
  starting transfers between devices  36.2 us (9%)
  matrix products  16.2 us (4%)
  between operations  15.1 us (4%)
  other arithmetic  8.27 us (2%)
    slice x50, local copies, waits for them, and re-layouts, body(): lax.associative_scan(chain_step, (decay, drive), axis=0)  56 us
    all_gather x1, waiting for transfers between devices, expert_down(): lax.all_gather(active, 'tp')  47.6 us
    all_to_all x1, waiting for transfers between devices, sum_at_owner(): lax.all_to_all(pieces, axis, split_axis=0, concat_axis=0, tiled=True)  47.3 us
    all_gather x1, waiting for transfers between devices, piecewise(): blocks = [lax.all_gather(slab, axis) for slab in pieces]  43.7 us
    pad x32, local copies, waits for them, and re-layouts, body(): lax.associative_scan(chain_step, (decay, drive), axis=0)  36.4 us
    all_to_all x1, blocking collectives, body(): lax.all_to_all(outgoing, 'sp', split_axis=0, concat_axis=0, tiled=True)  19.6 us
    all_to_all x1, blocking collectives, body(): lax.all_to_all(result.reshape(tp_size, experts * capacity, -1), 'tp', spl...  18.9 us
    all_to_all x1, waiting for transfers between devices, body(): lax.all_to_all(joined.reshape(experts, capacity, model_width), 'sp', spli...  17.4 us
  transfers between devices with their start and end apart: 6, of which 5 were waited for; matrix products, arithmetic and copies ran while one was open for 2% of the time, Pallas kernels for 0%

profile of v1, /device:TPU:1, one launch (start us, length us, event | category | flops | bytes accessed | tf_op | source)
XLA Modules:
  0.0 392.9 jit_solution(12222472088318258005)
XLA Ops:
  7.4 3.9 collective-permute-start
  13.9 1.1 copy.89
  18.9 4.5 %slice.371 = f32[256,128]{0,1:T(8,128)S(1)} slice(f32[512,128]{0,1:T(8,128)S(1)} %get-tuple-element.9), slice={[0:511:2], [0:128:1]} | slice | bytes 262144 | tf_op jit(solution)/shard_map/slice | solution.py:164
  23.4 4.5 %slice.372 = f32[256,128]{0,1:T(8,128)S(1)} slice(f32[512,128]{0,1:T(8,128)S(1)} %get-tuple-element.9), slice={[1:512:2], [0:128:1]} | slice | bytes 262144 | tf_op jit(solution)/shard_map/slice | solution.py:164
  27.9 4.5 %slice.370 = f32[256,128]{0,1:T(8,128)S(1)} slice(f32[512,128]{0,1:T(8,128)S(1)} %get-tuple-element.10), slice={[1:512:2], [0:128:1]} | slice | bytes 262144 | tf_op jit(solution)/shard_map/slice | solution.py:164
  32.4 5.0 %slice.374 = f32[256,128]{0,1:T(8,128)S(1)} slice(f32[512,128]{0,1:T(8,128)S(1)} %get-tuple-element.10), slice={[0:511:2], [0:128:1]} | slice | bytes 262144 | tf_op jit(solution)/shard_map/slice | solution.py:164
  37.4 2.2 slice.377
  39.7 2.2 slice.378
  41.9 2.2 slice.376
  44.1 2.2 slice.380
  46.3 1.1 slice.383
  47.5 1.2 slice.384
  48.6 1.2 slice.382
  49.8 1.1 slice.386
  60.3 1.1 slice.381
  61.5 1.1 slice.430
  62.6 2.2 slice.375
  64.8 2.2 slice.432
  67.0 4.5 %slice.369 = f32[255,128]{0,1:T(8,128)S(1)} slice(f32[512,128]{0,1:T(8,128)S(1)} %get-tuple-element.10), slice={[2:512:2], [0:128:1]} | slice | bytes 261120 | tf_op jit(solution)/shard_map/slice | solution.py:164
  71.5 4.9 %slice.434 = f32[255,128]{0,1:T(8,128)S(1)} slice(f32[512,128]{0,1:T(8,128)S(1)} %get-tuple-element.9), slice={[2:512:2], [0:128:1]} | slice | bytes 261120 | tf_op jit(solution)/shard_map/slice | solution.py:164
  84.9 1.1 pad.140
  86.0 1.1 pad.141
  87.1 1.1 pad.123
  88.4 1.1 pad.122
  89.7 2.2 pad.142
  91.9 2.2 pad.143
  94.1 4.5 %pad.145 = f32[512,128]{0,1:T(8,128)S(1)} pad(f32[256,128]{0,1:T(8,128)S(1)} %add.346, f32[]{:T(128)} %constant.25.clone.1), padding=1_0_1x0_0_0 | pad | bytes 393220 | tf_op jit(solution)/shard_map/pad | solution.py:164
  98.7 2.2 pad.124
  100.9 2.2 pad.125
  103.3 4.4 %pad.144 = f32[512,128]{0,1:T(8,128)S(1)} pad(f32[256,128]{0,1:T(8,128)S(1)} %pad_maximum_fusion.1, f32[]{:T(128)} %constant.25.clone.1), padding=0_1_1x0_0_0 | pad | bytes 393220 | tf_op jit(solution)/shard_map/pad | solution.py:164
  107.9 4.6 %pad.127 = f32[512,128]{0,1:T(8,128)S(1)} pad(f32[256,128]{0,1:T(8,128)S(1)} %add.336, f32[]{:T(128)} %constant.25.clone.1), padding=1_0_1x0_0_0 | pad | bytes 393220 | tf_op jit(solution)/shard_map/pad | solution.py:164
  112.5 4.4 %pad.126 = f32[512,128]{0,1:T(8,128)S(1)} pad(f32[256,128]{0,1:T(8,128)S(1)} %pad_maximum_fusion, f32[]{:T(128)} %constant.25.clone.1), padding=0_1_1x0_0_0 | pad | bytes 393220 | tf_op jit(solution)/shard_map/pad | solution.py:164
  117.7 12.6 %all-to-all-start = ((f32[32,2,128]{2,1,0:T(2,128)}), f32[32,2,128]{2,1,0:T(2,128)S(1)}, u32[]{:S(2)}, u32[]{:S(2)}) async-start(f32[32,2,128]{2,1,0:T(2,128)} %broadcast_in_dim.64), calls=%async_computation | async-start | bytes 65536 | tf_op jit(solution)/shard_map/all_to_all | solution.py:18
  130.4 8.7 %all-to-all-done = f32[32,2,128]{2,1,0:T(2,128)S(1)} async-done(((f32[32,2,128]{2,1,0:T(2,128)}), f32[32,2,128]{2,1,0:T(2,128)S(1)}, u32[]{:S(2)}, u32[]{:S(2)}) %all-to-all-start) | async-done | bytes 32800 | tf_op jit(solution)/shard_map/all_to_all | solution.py:18
  139.5 2.2 convolution_convert_fusion
  141.7 9.5 %all-to-all-start.1 = ((bf16[16,32,2048]{2,1,0:T(8,128)(2,1)}), bf16[16,32,2048]{2,1,0:T(8,128)(2,1)S(1)}, u32[]{:S(2)}, u32[]{:S(2)}) async-start(bf16[16,32,2048]{2,1,0:T(8,128)(2,1)} %bitcast.12), calls=%async_computation.1 | async-start | bytes 4194304 | tf_op jit(solution)/shard_map/all_to_all | solution.py:67
  152.9 47.3 %all-to-all-done.1 = bf16[16,32,2048]{2,1,0:T(8,128)(2,1)S(1)} async-done(((bf16[16,32,2048]{2,1,0:T(8,128)(2,1)}), bf16[16,32,2048]{2,1,0:T(8,128)(2,1)S(1)}, u32[]{:S(2)}, u32[]{:S(2)}) %all-to-all-start.1) | async-done | bytes 2097184 | tf_op jit(solution)/shard_map/all_to_all | solution.py:67
  202.2 19.6 %all_to_all.35 = bf16[32,3,2048]{2,1,0:T(4,128)(2,1)S(1)} all-to-all(bf16[32,3,2048]{2,1,0:T(4,128)(2,1)S(1)} %broadcast_select_fusion), channel_id=1, replica_groups=mesh['sp'=32,'tp'=16] {'sp'}, dimensions={0} | all-to-all | bytes 786432 | tf_op jit(solution)/shard_map/all_to_all | solution.py:195
  221.9 1.1 all_gather_reshape.3
  223.3 43.7 %all-gather.3.cloned.1.call-done = bf16[16,1,96,2048]{3,2,1,0:T(8,128)(2,1)} async-done(((bf16[1,1,96,2048]{3,2,1,0:T(8,128)(2,1)}), bf16[16,1,96,2048]{3,2,1,0:T(8,128)(2,1)}) %all-gather.3.cloned.1.call-update) | async-done | bytes 6291472 | tf_op jit(solution)/shard_map/all_gather | solution.py:81
  266.9 4.7 %fusion.2 = f32[16,96,128]{2,1,0:T(8,128)S(1)} fusion(bf16[16,1,96,2048]{3,2,1,0:T(8,128)(2,1)} %all-gather.3.cloned.1.call-done, bf16[1,2048,128]{2,1,0:T(8,128)(2,1)S(1)} %copy-done.5), kind=kOutput, calls=%fused_computation.4 | convolution fusion | flops 805306368 | bytes 7602176 | tf_op jit(solution)/shard_map/vmap()/dot_general | solution.py:105
  271.7 2.6 fusion.7
  274.3 47.6 %all-gather.5.cloned.1.call-done = bf16[16,1536,128]{2,1,0:T(8,128)(2,1)} async-done(((bf16[1,1536,128]{2,1,0:T(8,128)(2,1)}), bf16[16,1536,128]{2,1,0:T(8,128)(2,1)}) %all-gather.5.cloned.1.call-update) | async-done | bytes 6291472 | tf_op jit(solution)/shard_map/all_gather | solution.py:113
  321.9 8.6 %copy.107 = bf16[16,1536,128]{1,2,0:T(8,128)(2,1)} copy(bf16[16,1536,128]{2,1,0:T(8,128)(2,1)} %all-gather.5.cloned.1.call-done) | data formatting | bytes 12582912 | tf_op jit(solution)/shard_map/all_gather | solution.py:113
  330.6 4.6 %convolution_convert_fusion.1 = bf16[1536,128]{1,0:T(8,128)(2,1)S(1)} fusion(bf16[1536,2048]{0,1:T(8,128)(2,1)} %bitcast.88, bf16[1,2048,128]{2,1,0:T(8,128)(2,1)S(1)} %copy-done.7), kind=kOutput, calls=%fused_computation.8 | convolution fusion | flops 805502976 | bytes 7208960 | tf_op jit(solution)/shard_map/dot_general | solution.py:112
  335.2 18.9 %all_to_all.36 = bf16[16,96,128]{2,1,0:T(8,128)(2,1)S(1)} all-to-all(bf16[16,96,128]{2,1,0:T(8,128)(2,1)S(1)} %bitcast.101), channel_id=1, replica_groups=mesh['sp'=32,'tp'=16] {'tp'}, dimensions={0} | all-to-all | bytes 786432 | tf_op jit(solution)/shard_map/all_to_all | solution.py:207
  355.2 9.9 %all-to-all-start.4 = ((bf16[32,3,2048]{2,1,0:T(4,128)(2,1)}), bf16[32,3,2048]{2,1,0:T(4,128)(2,1)S(1)}, u32[]{:S(2)}, u32[]{:S(2)}) async-start(bf16[32,3,2048]{2,1,0:T(4,128)(2,1)} %reshape.156), calls=%async_computation.4 | async-start | bytes 1048576 | tf_op jit(solution)/shard_map/all_to_all | solution.py:214
  365.4 17.4 %all-to-all-done.4 = bf16[32,3,2048]{2,1,0:T(4,128)(2,1)S(1)} async-done(((bf16[32,3,2048]{2,1,0:T(4,128)(2,1)}), bf16[32,3,2048]{2,1,0:T(4,128)(2,1)S(1)}, u32[]{:S(2)}, u32[]{:S(2)}) %all-to-all-start.4) | async-done | bytes 393248 | tf_op jit(solution)/shard_map/all_to_all | solution.py:214
  (208 shorter events, 34.9 us)
Async XLA Ops:
  6.5 133.0 %copy-start = (bf16[128,2048]{1,0:T(8,128)(2,1)S(1)}, bf16[128,2048]{1,0:T(8,128)(2,1)}, u32[]{:S(2)}) copy-start(bf16[128,2048]{1,0:T(8,128)(2,1)} %param.23) | copy-start | bytes 1572868
  7.4 8.6 %collective-permute-start = (bf16[3,128]{0,1:T(8,128)(2,1)S(1)}, bf16[3,128]{0,1:T(8,128)(2,1)S(1)}, u32[]{:S(2)}, u32[]{:S(2)}) collective-permute-start(bf16[3,128]{0,1:T(8,128)(2,1)S(1)} %copy.86), channel_id=1, source_target_pairs={{0,16},{16,32},{32,48},{48,64},{64,80},{80,96},{96,112},{112,128},... | collective-permute-start | bytes 2312 | tf_op jit(solution)/shard_map/ppermute | solution.py:13
  107.8 92.8 %copy-start.1 = (bf16[32,2048]{1,0:T(8,128)(2,1)S(1)}, bf16[32,2048]{1,0:T(8,128)(2,1)}, u32[]{:S(2)}) copy-start(bf16[32,2048]{1,0:T(8,128)(2,1)} %param.15) | copy-start | bytes 393220
  112.4 88.3 %copy-start.2 = (f32[2048]{0:T(1024)S(1)}, f32[2048]{0:T(1024)}, u32[]{:S(2)}) copy-start(f32[2048]{0:T(1024)} %param.24) | copy-start | bytes 24580
  117.7 21.3 %all-to-all-start = ((f32[32,2,128]{2,1,0:T(2,128)}), f32[32,2,128]{2,1,0:T(2,128)S(1)}, u32[]{:S(2)}, u32[]{:S(2)}) async-start(f32[32,2,128]{2,1,0:T(2,128)} %broadcast_in_dim.64), calls=%async_computation | async-start | bytes 65536 | tf_op jit(solution)/shard_map/all_to_all | solution.py:18
  141.7 58.5 %all-to-all-start.1 = ((bf16[16,32,2048]{2,1,0:T(8,128)(2,1)}), bf16[16,32,2048]{2,1,0:T(8,128)(2,1)S(1)}, u32[]{:S(2)}, u32[]{:S(2)}) async-start(bf16[16,32,2048]{2,1,0:T(8,128)(2,1)} %bitcast.12), calls=%async_computation.1 | async-start | bytes 4194304 | tf_op jit(solution)/shard_map/all_to_all | solution.py:67
  151.2 115.8 %copy-start.5 = (bf16[1,2048,128]{2,1,0:T(8,128)(2,1)S(1)}, bf16[1,2048,128]{2,1,0:T(8,128)(2,1)}, u32[]{:S(2)}) copy-start(bf16[1,2048,128]{2,1,0:T(8,128)(2,1)} %param.27) | copy-start | bytes 1572868
  151.2 115.8 %all-gather.3.cloned.1.call-start = ((), (), s32[]{:S(2)}) async-start(), calls=%async_computation.5 | async-start | bytes 6684672 | tf_op jit(solution)/shard_map/all_gather | solution.py:81
  222.9 48.7 %copy-start.6 = (bf16[1,2048,128]{2,1,0:T(8,128)(2,1)S(1)}, bf16[1,2048,128]{2,1,0:T(8,128)(2,1)}, u32[]{:S(2)}) copy-start(bf16[1,2048,128]{2,1,0:T(8,128)(2,1)} %param.28) | copy-start | bytes 1572868
  223.0 99.0 %all-gather.5.cloned.1.call-start = ((), (), s32[]{:S(2)}) async-start(), calls=%async_computation.6 | async-start | bytes 6684672 | tf_op jit(solution)/shard_map/all_gather | solution.py:113
  266.9 4.8 %copy-start.4 = (bf16[16,1,96,2048]{3,2,1,0:T(8,128)(2,1)S(1)}, bf16[16,1,96,2048]{3,2,1,0:T(8,128)(2,1)}, u32[]{:S(2)}) copy-start(bf16[16,1,96,2048]{3,2,1,0:T(8,128)(2,1)} %all-gather.3.cloned.1.call-done) | copy-start | bytes 18874372
  274.3 56.3 %copy-start.7 = (bf16[1,2048,128]{2,1,0:T(8,128)(2,1)S(1)}, bf16[1,2048,128]{2,1,0:T(8,128)(2,1)}, u32[]{:S(2)}) copy-start(bf16[1,2048,128]{2,1,0:T(8,128)(2,1)} %param.29) | copy-start | bytes 1572868
  330.6 34.7 %copy-start.3 = (f32[32,2]{0,1:T(2,128)S(1)}, f32[32,2]{0,1:T(2,128)}, u32[]{:S(2)}) copy-start(f32[32,2]{0,1:T(2,128)} %param.26) | copy-start | bytes 772
  355.2 27.6 %all-to-all-start.4 = ((bf16[32,3,2048]{2,1,0:T(4,128)(2,1)}), bf16[32,3,2048]{2,1,0:T(4,128)(2,1)S(1)}, u32[]{:S(2)}, u32[]{:S(2)}) async-start(bf16[32,3,2048]{2,1,0:T(4,128)(2,1)} %reshape.156), calls=%async_computation.4 | async-start | bytes 1048576 | tf_op jit(solution)/shard_map/all_to_all | solution.py:214
Sparse Core Ops, SparseCore 0:
  223.1 43.8 all-gather.2
  274.4 47.4 all-gather.4
